TPU v7x, 32 devices: a whole 2x2x4 slice. The times are simulated.
32 devices in a mesh: grp: 2 (over y), fs: 4 (over z), tp: 4 (over x, core).
Axes of the slice: x: 2, y: 2, z: 4, core: 2. Of those that a mesh axis runs over, the one named last changes fastest.
Arguments:
- tokens: bfloat16 [3072, 2048], P(('grp', 'fs'), 'tp'), parts along dimension 0, may hold values from -6 to 6
- mix_gain: float32 [2048], replicated, may hold values from 0.1 to 1.9
- w_signal: bfloat16 [2048, 1024], P('fs', 'tp'), may hold values from -0.125 to 0.125
- w_outer_gate: bfloat16 [2048, 1024], P('fs', 'tp'), may hold values from -0.125 to 0.125
- w_inner_gate: bfloat16 [2048, 1024], P('fs', 'tp'), may hold values from -0.125 to 0.125
- mix_taps: float32 [3, 1024], P(None, 'tp'), may hold values from -3 to 3
- w_mix_out: bfloat16 [1024, 2048], P('tp', 'fs'), may hold values from -0.1875 to 0.1875
- ffn_gain: float32 [2048], replicated, may hold values from 0.1 to 1.9
- w_gate: bfloat16 [2048, 5120], P('fs', 'tp'), may hold values from -0.125 to 0.125
- w_value: bfloat16 [2048, 5120], P('fs', 'tp'), may hold values from -0.125 to 0.125
- up_taps: float32 [2, 3, 5120], P(None, None, 'tp'), may hold values from -3 to 3
- up_bias: float32 [2, 5120], P(None, 'tp'), may hold values from -3 to 3
- w_down: bfloat16 [5120, 2048], P('tp', 'fs'), may hold values from -0.078125 to 0.078125
Outputs:
- layer_out: bfloat16 [3072, 2048], P(('grp', 'fs'), 'tp'), parts along dimension 0
There are 2 independent parts, one for each index of `grp`. A program takes and returns all parts, laid end to end along the dimension named above; an argument that names none is the same for every part. Nothing has to cross between parts.
All inputs are finite; a program needn't handle non-finite values.
Results may differ from a plain program's by a relative error of at most 0.022.
Values may be sent and summed in bfloat16 or wider, within the bound.
A program may use at most 64 MiB of HBM per device.

v0:
```python
import jax
import jax.numpy as jnp
from jax import lax
from jax.sharding import PartitionSpec as P

SEQS_DEV = 2


def conv_positions(values, taps):
    width = values.shape[1]
    blocks = values.reshape(SEQS_DEV, -1, width)
    length = blocks.shape[1]
    padded = jnp.pad(blocks, ((0, 0), (2, 0), (0, 0)))
    result = (
        padded[:, 0:length] * taps[0]
        + padded[:, 1 : length + 1] * taps[1]
        + padded[:, 2 : length + 2] * taps[2]
    )
    return result.reshape(-1, width)


def rms_norm(stream, gain):
    values = stream.astype(jnp.float32)
    scale = lax.rsqrt(jnp.mean(values * values, axis=-1, keepdims=True) + 1e-06)
    return (values * scale * gain).astype(jnp.bfloat16)


def on_device(
    tokens,
    mix_gain,
    w_signal,
    w_outer_gate,
    w_inner_gate,
    mix_taps,
    w_mix_out,
    ffn_gain,
    w_gate,
    w_value,
    up_taps,
    up_bias,
    w_down,
):
    whole = lax.all_gather(tokens, "tp", axis=1, tiled=True)
    normed = rms_norm(whole, mix_gain)
    pieces = (
        lax.all_gather(w_signal, "fs", axis=0, tiled=True),
        lax.all_gather(w_outer_gate, "fs", axis=0, tiled=True),
        lax.all_gather(w_inner_gate, "fs", axis=0, tiled=True),
    )
    columns = normed
    signal, outer, inner = tuple(
        (jnp.dot(columns, piece, preferred_element_type=jnp.float32) for piece in pieces)
    )
    signal = signal.astype(jnp.bfloat16).astype(jnp.float32)
    outer = outer.astype(jnp.bfloat16).astype(jnp.float32)
    inner = inner.astype(jnp.bfloat16).astype(jnp.float32)
    mixed = (outer * conv_positions(inner * signal, mix_taps)).astype(jnp.bfloat16)
    mix_terms = jnp.dot(
        mixed,
        lax.all_gather(w_mix_out, "fs", axis=1, tiled=True),
        preferred_element_type=jnp.float32,
    )
    mix_sum = lax.psum_scatter(
        mix_terms.astype(jnp.bfloat16), "tp", scatter_dimension=1, tiled=True
    ).astype(jnp.float32)
    resid = (tokens.astype(jnp.float32) + mix_sum).astype(jnp.bfloat16)
    whole_ffn = lax.all_gather(resid, "tp", axis=1, tiled=True)
    normed_ffn = rms_norm(whole_ffn, ffn_gain)
    pieces = (
        lax.all_gather(w_gate, "fs", axis=0, tiled=True),
        lax.all_gather(w_value, "fs", axis=0, tiled=True),
    )
    columns = normed_ffn
    gate = jnp.dot(columns, pieces[0], preferred_element_type=jnp.float32)
    value = jnp.dot(columns, pieces[1], preferred_element_type=jnp.float32)
    gate = gate.astype(jnp.bfloat16).astype(jnp.float32)
    value = value.astype(jnp.bfloat16).astype(jnp.float32)
    gate_conv = conv_positions(gate, up_taps[0]) + up_bias[0]
    value_conv = conv_positions(value, up_taps[1]) + up_bias[1]
    hidden = (jax.nn.silu(gate_conv) * value_conv).astype(jnp.bfloat16)
    ffn_terms = jnp.dot(
        hidden, lax.all_gather(w_down, "fs", axis=1, tiled=True), preferred_element_type=jnp.float32
    )
    ffn_sum = lax.psum_scatter(
        ffn_terms.astype(jnp.bfloat16), "tp", scatter_dimension=1, tiled=True
    ).astype(jnp.float32)
    return (resid.astype(jnp.float32) + ffn_sum).astype(jnp.bfloat16)


def solution(mesh):
    placed = (
        P(("grp", "fs"), "tp"),
        P(),
        P("fs", "tp"),
        P("fs", "tp"),
        P("fs", "tp"),
        P(None, "tp"),
        P("tp", "fs"),
        P(),
        P("fs", "tp"),
        P("fs", "tp"),
        P(None, None, "tp"),
        P(None, "tp"),
        P("tp", "fs"),
    )
    return jax.shard_map(
        on_device, mesh=mesh, in_specs=placed, out_specs=P(("grp", "fs"), "tp"), check_vma=False
    )
```

profile of v0, /device:TPU:0, one launch (start us, length us, event | category | flops | bytes accessed | tf_op | source)
XLA Modules:
  0.0 537.4 jit_solution(5827497235861300328)
XLA Ops:
  6.5 0.7 all-gather.10.cloned.1.call-update
  10.0 0.8 fusion.32
  10.8 20.5 %all-gather.10.cloned.1.call-done = bf16[384,2048]{1,0:T(8,128)(2,1)} async-done(((bf16[384,512]{1,0:T(8,128)(2,1)}), bf16[384,2048]{1,0:T(8,128)(2,1)}) %all-gather.10.cloned.1.call-update) | async-done | bytes 1572880 | tf_op jit(solution)/shard_map/all_gather | solution.py:43
  31.3 1.8 fusion
  33.1 27.8 %all-gather.14.cloned.1.call-done = bf16[2048,256]{1,0:T(8,128)(2,1)} async-done(((bf16[512,256]{1,0:T(8,128)(2,1)}), bf16[2048,256]{1,0:T(8,128)(2,1)}) %all-gather.14.cloned.1.call-update) | async-done | bytes 1048592 | tf_op jit(solution)/shard_map/all_gather | solution.py:48
  60.9 2.3 fusion.18
  63.2 26.6 %all-gather.16.cloned.1.call-done = bf16[2048,256]{1,0:T(8,128)(2,1)} async-done(((bf16[512,256]{1,0:T(8,128)(2,1)}), bf16[2048,256]{1,0:T(8,128)(2,1)}) %all-gather.16.cloned.1.call-update) | async-done | bytes 1048592 | tf_op jit(solution)/shard_map/all_gather | solution.py:46
  89.8 1.8 fusion.17
  91.8 26.8 %all-gather.12.cloned.1.call-done = bf16[2048,256]{1,0:T(8,128)(2,1)} async-done(((bf16[512,256]{1,0:T(8,128)(2,1)}), bf16[2048,256]{1,0:T(8,128)(2,1)}) %all-gather.12.cloned.1.call-update) | async-done | bytes 1048592 | tf_op jit(solution)/shard_map/all_gather | solution.py:47
  118.6 28.8 %all-gather.18.cloned.1.call-done = bf16[256,2048]{1,0:T(8,128)(2,1)} async-done(((bf16[256,512]{1,0:T(8,128)(2,1)}), bf16[256,2048]{1,0:T(8,128)(2,1)}) %all-gather.18.cloned.1.call-update) | async-done | bytes 1048592 | tf_op jit(solution)/shard_map/all_gather | solution.py:60
  147.5 4.6 convolution_convert_fusion.3
  152.1 27.5 %reduce-scatter.3.cloned.1.call-done = bf16[384,512]{1,0:T(8,128)(2,1)} async-done(((bf16[384,2048]{1,0:T(8,128)(2,1)}), bf16[384,512]{1,0:T(8,128)(2,1)}) %reduce-scatter.3.cloned.1.call-update) | async-done | bytes 393232 | tf_op jit(solution)/shard_map/reduce_scatter | solution.py:63
  179.6 1.8 add_convert_fusion.1
  184.4 16.9 %all-gather.20.cloned.1.call-done = bf16[384,2048]{1,0:T(8,128)(2,1)} async-done(((bf16[384,512]{1,0:T(8,128)(2,1)}), bf16[384,2048]{1,0:T(8,128)(2,1)}) %all-gather.20.cloned.1.call-update) | async-done | bytes 1572880 | tf_op jit(solution)/shard_map/all_gather | solution.py:67
  201.3 1.8 fusion.3
  203.1 97.8 %all-gather.24.cloned.1.call-done = bf16[2048,1280]{1,0:T(8,128)(2,1)} async-done(((bf16[512,1280]{1,0:T(8,128)(2,1)}), bf16[2048,1280]{1,0:T(8,128)(2,1)}) %all-gather.24.cloned.1.call-update) | async-done | bytes 5242896 | tf_op jit(solution)/shard_map/all_gather | solution.py:71
  300.9 5.2 convolution_convert_fusion.1
  306.3 92.6 %all-gather.22.cloned.1.call-done = bf16[2048,1280]{1,0:T(8,128)(2,1)} async-done(((bf16[512,1280]{1,0:T(8,128)(2,1)}), bf16[2048,1280]{1,0:T(8,128)(2,1)}) %all-gather.22.cloned.1.call-update) | async-done | bytes 5242896 | tf_op jit(solution)/shard_map/all_gather | solution.py:70
  398.9 4.8 convolution_convert_fusion.2
  404.4 1.2 fusion.8
  406.2 90.5 %all-gather.26.cloned.1.call-done = bf16[1280,2048]{1,0:T(8,128)(2,1)} async-done(((bf16[1280,512]{1,0:T(8,128)(2,1)}), bf16[1280,2048]{1,0:T(8,128)(2,1)}) %all-gather.26.cloned.1.call-update) | async-done | bytes 5242896 | tf_op jit(solution)/shard_map/all_gather | solution.py:82
  496.7 5.9 %convolution_convert_fusion = bf16[384,2048]{1,0:T(8,128)(2,1)} fusion(bf16[384,1280]{1,0:T(8,128)(2,1)S(1)} %fusion.15, bf16[1280,2048]{1,0:T(8,128)(2,1)} %all-gather.26.cloned.1.call-done), kind=kOutput, calls=%fused_computation.10 | convolution fusion | flops 2014052352 | bytes 7798784 | tf_op jit(solution)/shard_map/dot_general | solution.py:81
  502.6 26.5 %reduce-scatter.5.cloned.1.call-done = bf16[384,512]{1,0:T(8,128)(2,1)} async-done(((bf16[384,2048]{1,0:T(8,128)(2,1)}), bf16[384,512]{1,0:T(8,128)(2,1)}) %reduce-scatter.5.cloned.1.call-update) | async-done | bytes 393232 | tf_op jit(solution)/shard_map/reduce_scatter | solution.py:84
  529.1 1.8 add_convert_fusion
  (59 shorter events, 7.1 us)
Async XLA Ops:
  6.5 54.3 %copy-start.13 = (f32[2048]{0:T(1024)S(1)}, f32[2048]{0:T(1024)}, u32[]{:S(2)}) copy-start(f32[2048]{0:T(1024)} %param.14) | copy-start | bytes 24580
  6.5 24.7 %all-gather.10.cloned.1.call-start = ((), (), s32[]{:S(2)}) async-start(), calls=%async_computation.2 | async-start | bytes 1966080 | tf_op jit(solution)/shard_map/all_gather | solution.py:43
  7.3 53.6 %all-gather.14.cloned.1.call-start = ((), (), s32[]{:S(2)}) async-start(), calls=%async_computation.4 | async-start | bytes 1310720 | tf_op jit(solution)/shard_map/all_gather | solution.py:48
  8.0 81.8 %all-gather.16.cloned.1.call-start = ((), (), s32[]{:S(2)}) async-start(), calls=%async_computation.5 | async-start | bytes 1310720 | tf_op jit(solution)/shard_map/all_gather | solution.py:46
  8.7 109.9 %all-gather.12.cloned.1.call-start = ((), (), s32[]{:S(2)}) async-start(), calls=%async_computation.3 | async-start | bytes 1310720 | tf_op jit(solution)/shard_map/all_gather | solution.py:47
  9.3 138.1 %all-gather.18.cloned.1.call-start = ((), (), s32[]{:S(2)}) async-start(), calls=%async_computation.6 | async-start | bytes 1310720 | tf_op jit(solution)/shard_map/all_gather | solution.py:60
  9.9 169.7 %reduce-scatter.3.cloned.1.call-start = ((), (), s32[]{:S(2)}) async-start(), calls=%async_computation.7 | async-start | bytes 1966080 | tf_op jit(solution)/shard_map/reduce_scatter | solution.py:63
  33.1 56.8 %copy-start.1 = (bf16[384,2048]{1,0:T(8,128)(2,1)S(1)}, bf16[384,2048]{1,0:T(8,128)(2,1)}, u32[]{:S(2)}) copy-start(bf16[384,2048]{1,0:T(8,128)(2,1)} %all-gather.10.cloned.1.call-done) | copy-start | bytes 4718596
  147.5 32.2 %copy-start.3 = (bf16[384,512]{1,0:T(8,128)(2,1)S(1)}, bf16[384,512]{1,0:T(8,128)(2,1)}, u32[]{:S(2)}) copy-start(bf16[384,512]{1,0:T(8,128)(2,1)} %param.13) | copy-start | bytes 1179652
  152.1 49.2 %all-gather.20.cloned.1.call-start = ((), (), s32[]{:S(2)}) async-start(), calls=%async_computation.8 | async-start | bytes 1966080 | tf_op jit(solution)/shard_map/all_gather | solution.py:67
  181.5 2.2 copy-start.11
  181.5 2.2 copy-start.10
  181.5 119.4 %all-gather.24.cloned.1.call-start = ((), (), s32[]{:S(2)}) async-start(), calls=%async_computation.10 | async-start | bytes 6553600 | tf_op jit(solution)/shard_map/all_gather | solution.py:71
  182.3 118.7 %copy-start.14 = (f32[2048]{0:T(1024)S(1)}, f32[2048]{0:T(1024)}, u32[]{:S(2)}) copy-start(f32[2048]{0:T(1024)} %param.20) | copy-start | bytes 24580
  182.3 216.6 %all-gather.22.cloned.1.call-start = ((), (), s32[]{:S(2)}) async-start(), calls=%async_computation.9 | async-start | bytes 6553600 | tf_op jit(solution)/shard_map/all_gather | solution.py:70
  183.0 313.7 %all-gather.26.cloned.1.call-start = ((), (), s32[]{:S(2)}) async-start(), calls=%async_computation.11 | async-start | bytes 6553600 | tf_op jit(solution)/shard_map/all_gather | solution.py:82
  183.6 345.5 %reduce-scatter.5.cloned.1.call-start = ((), (), s32[]{:S(2)}) async-start(), calls=%async_computation.12 | async-start | bytes 1966080 | tf_op jit(solution)/shard_map/reduce_scatter | solution.py:84
  203.1 103.1 %copy-start.12 = (f32[384]{0:T(512)}, f32[384]{0:T(512)S(1)}, u32[]{:S(2)}) copy-start(f32[384]{0:T(512)S(1)} %add_rsqrt_fusion) | copy-start | bytes 4612
  306.1 92.8 %copy-start.2 = (bf16[384,2048]{1,0:T(8,128)(2,1)S(1)}, bf16[384,2048]{1,0:T(8,128)(2,1)}, u32[]{:S(2)}) copy-start(bf16[384,2048]{1,0:T(8,128)(2,1)} %all-gather.20.cloned.1.call-done) | copy-start | bytes 4718596
  403.7 0.7 copy-start.6
  403.7 0.7 copy-start.7
  403.7 0.7 copy-start.8
  403.7 0.7 copy-start.9
  406.2 122.9 %copy-start = (bf16[384,512]{1,0:T(8,128)(2,1)S(1)}, bf16[384,512]{1,0:T(8,128)(2,1)}, u32[]{:S(2)}) copy-start(bf16[384,512]{1,0:T(8,128)(2,1)} %add_convert_fusion.1) | copy-start | bytes 1179652
  (2 other events, 1.4 us)
Sparse Core Ops, SparseCore 0:
  8.9 22.3 all-gather.9
  32.8 27.9 all-gather.13
  62.4 27.3 all-gather.15
  91.3 27.3 all-gather.11
  120.1 27.3 all-gather.17
  152.2 27.3 reduce-scatter.2
  181.6 19.6 all-gather.19
  202.8 98.0 all-gather.23
  302.5 96.3 all-gather.21
  400.3 96.3 all-gather.25
  502.7 26.3 reduce-scatter.4
where the time goes:
time: 538 us; the launch traced here: 537 us
  waiting for transfers between devices  488 us (91%)
  matrix products  24.6 us (5%)
  between operations  13.4 us (2%)
  other arithmetic  9.39 us (2%)
    all_gather x1, waiting for transfers between devices, on_device(): lax.all_gather(w_value, 'fs', axis=0, tiled=True)  97.8 us
    all_gather x1, waiting for transfers between devices, on_device(): lax.all_gather(w_gate, 'fs', axis=0, tiled=True)  92.6 us
    all_gather x1, waiting for transfers between devices, on_device(): lax.all_gather(w_down, 'fs', axis=1, tiled=True)  90.5 us
    all_gather x1, waiting for transfers between devices, on_device(): lax.all_gather(w_mix_out, 'fs', axis=1, tiled=True)  28.8 us
    all_gather x1, waiting for transfers between devices, on_device(): lax.all_gather(w_inner_gate, 'fs', axis=0, tiled=True)  27.8 us
    reduce_scatter x1, waiting for transfers between devices, on_device(): lax.psum_scatter(mix_terms.astype(jnp.bfloat16), 'tp', scatter_dimension=...  27.5 us
    all_gather x1, waiting for transfers between devices, on_device(): lax.all_gather(w_outer_gate, 'fs', axis=0, tiled=True)  26.8 us
    all_gather x1, waiting for transfers between devices, on_device(): lax.all_gather(w_signal, 'fs', axis=0, tiled=True)  26.6 us
  transfers between devices with their start and end apart: 11, of which 11 were waited for; matrix products, arithmetic and copies ran while one was open for 4% of the time, Pallas kernels for 0%

commit v1 on v0

--- a/solution.py
+++ b/solution.py
@@ -1,6 +1,10 @@
+import functools
+
 import jax
 import jax.numpy as jnp
 from jax import lax
+from jax.experimental import pallas as pl
+from jax.experimental.pallas import tpu as pltpu
 from jax.sharding import PartitionSpec as P
 
 SEQS_DEV = 2
@@ -87,7 +91,394 @@
     return (resid.astype(jnp.float32) + ffn_sum).astype(jnp.bfloat16)
 
 
+MESH = pl.DeviceIdType.MESH
+UP, DOWN = 0, 1
+
+
+def shifted(values, by, length):
+    rolled = pltpu.roll(values, by, 0)
+    position = lax.rem(lax.broadcasted_iota(jnp.int32, values.shape, 0), length)
+    return jnp.where(position < by, 0.0, rolled)
+
+
+def conv_rows(values, taps, length):
+    return (
+        shifted(values, 2, length) * taps[0:1]
+        + shifted(values, 1, length) * taps[1:2]
+        + values * taps[2:3]
+    )
+
+
+def layer_kernel(
+    n_fs,
+    n_tp,
+    tokens,
+    mix_gain,
+    w_signal,
+    w_outer_gate,
+    w_inner_gate,
+    mix_taps,
+    w_mix_out,
+    ffn_gain,
+    w_gate,
+    w_value,
+    up_taps,
+    up_bias,
+    w_down,
+    out,
+    mix_in,
+    mix_out,
+    ffn_in,
+    ffn_out,
+    tok,
+    res,
+    normed,
+    total,
+    part,
+    got,
+    part_ffn,
+    got_ffn,
+    z_send,
+    z_recv,
+    y_send,
+    y_recv,
+    load_sem,
+    tp_send,
+    tp_recv,
+):
+    g, j, k = lax.axis_index("grp"), lax.axis_index("fs"), lax.axis_index("tp")
+    rows, own_cols = tokens.shape
+    length = rows // SEQS_DEV
+    shard, chans = w_signal.shape
+    half, half_chans = shard // 2, chans // 2
+    stages = 1 + w_gate.shape[1] // chans
+
+    def views(s, source, side):
+        at_rows = pl.ds(pl.multiple_of((source * 2 + side) * half, half), half)
+        at_chans = pl.ds(pl.multiple_of(side * half_chans, half_chans), half_chans)
+        if isinstance(s, int) and s == 0:
+            return mix_in.at[:, at_rows, :], mix_out.at[source, at_chans, :]
+        return ffn_in.at[s - 1, :, at_rows, :], ffn_out.at[s - 1, source, at_chans, :]
+
+    def z_copies(s, source, way):
+        to = j + 1 if way == UP else j - 1
+        return [
+            pltpu.make_async_remote_copy(
+                src_ref=view,
+                dst_ref=view,
+                send_sem=z_send.at[way, 2 * s + p, source],
+                recv_sem=z_recv.at[2 * s + p, source],
+                device_id={"fs": to},
+                device_id_type=MESH,
+            )
+            for p, view in enumerate(views(s, source, g))
+        ]
+
+    def y_copies(s, source, side):
+        return [
+            pltpu.make_async_remote_copy(
+                src_ref=view,
+                dst_ref=view,
+                send_sem=y_send.at[2 * s + p, source],
+                recv_sem=y_recv.at[2 * s + p, source],
+                device_id={"grp": 1 - g},
+                device_id_type=MESH,
+            )
+            for p, view in enumerate(views(s, source, side))
+        ]
+
+    def start(copies):
+        for copy in copies:
+            copy.start()
+
+    def own(s, way):
+        start(z_copies(s, j, way))
+
+    def relay(s, last):
+        for d in range(1, n_fs):
+
+            @pl.when(j - d >= 0)
+            def _():
+                for copy in z_copies(s, j - d, UP):
+                    copy.wait_recv()
+
+                @pl.when(j + 1 < n_fs)
+                def _():
+                    start(z_copies(s, j - d, UP))
+
+                start(y_copies(s, j - d, g))
+
+            @pl.when(j + d < n_fs)
+            def _():
+                for copy in z_copies(s, j + d, DOWN):
+                    copy.wait_recv()
+
+                @pl.when(j >= 1)
+                def _():
+                    start(z_copies(s, j + d, DOWN))
+
+                start(y_copies(s, j + d, g))
+
+            if not last:
+
+                @pl.when((j == d) & (j + 1 < n_fs))
+                def _():
+                    own(s + 1, UP)
+
+                @pl.when((n_fs - 1 - j == d) & (j >= 1))
+                def _():
+                    own(s + 1, DOWN)
+
+    def arrived(s):
+        for d in range(1, n_fs):
+            for copy in y_copies(s, lax.rem(j + d, n_fs), 1 - g):
+                copy.wait_recv()
+
+    def tp_copy(phase, d, src, dst, to):
+        return pltpu.make_async_remote_copy(
+            src_ref=src,
+            dst_ref=dst,
+            send_sem=tp_send.at[phase, d],
+            recv_sem=tp_recv.at[phase, d],
+            device_id={"tp": to},
+            device_id_type=MESH,
+        )
+
+    def gather_copy(phase, buffer, d):
+        return tp_copy(phase, d, buffer.at[k], buffer.at[k], lax.rem(k + d, n_tp))
+
+    def gather_wait(phase, buffer, d):
+        source = lax.rem(k + n_tp - d, n_tp)
+        tp_copy(phase, d, buffer.at[source], buffer.at[source], lax.rem(k + d, n_tp)).wait_recv()
+
+    def scatter_copy(phase, sent, received, d):
+        to = lax.rem(k + d, n_tp)
+        return tp_copy(phase, d, sent.at[to], received.at[d], to)
+
+    barrier = pltpu.get_barrier_semaphore()
+    for peer in (lax.rem(j + 1, n_fs), lax.rem(j + n_fs - 1, n_fs)):
+        pl.semaphore_signal(barrier, inc=1, device_id={"fs": peer}, device_id_type=MESH)
+    pl.semaphore_signal(barrier, inc=1, device_id={"grp": 1 - g}, device_id_type=MESH)
+    for d in range(1, n_tp):
+        pl.semaphore_signal(
+            barrier, inc=1, device_id={"tp": lax.rem(k + d, n_tp)}, device_id_type=MESH
+        )
+
+    at_rows = pl.ds(pl.multiple_of(j * shard, shard), shard)
+    loads = [
+        pltpu.make_async_copy(ref, mix_in.at[i, at_rows, :], load_sem.at[i])
+        for i, ref in enumerate((w_signal, w_outer_gate, w_inner_gate))
+    ]
+    loads.append(pltpu.make_async_copy(w_mix_out, mix_out.at[j], load_sem.at[3]))
+    loads.append(pltpu.make_async_copy(tokens, tok.at[k], load_sem.at[4]))
+    for s in range(1, stages):
+        cut = pl.ds((s - 1) * chans, chans)
+        base = 5 + 3 * (s - 1)
+        loads.append(
+            pltpu.make_async_copy(
+                w_gate.at[:, cut], ffn_in.at[s - 1, 0, at_rows, :], load_sem.at[base]
+            )
+        )
+        loads.append(
+            pltpu.make_async_copy(
+                w_value.at[:, cut], ffn_in.at[s - 1, 1, at_rows, :], load_sem.at[base + 1]
+            )
+        )
+        loads.append(
+            pltpu.make_async_copy(
+                w_down.at[cut, :], ffn_out.at[s - 1, j], load_sem.at[base + 2]
+            )
+        )
+    start(loads)
+    for copy in loads[:5]:
+        copy.wait()
+    pl.semaphore_wait(barrier, 3 + n_tp - 1)
+
+    @pl.when(j + 1 < n_fs)
+    def _():
+        own(0, UP)
+
+    @pl.when(j >= 1)
+    def _():
+        own(0, DOWN)
+
+    for d in range(1, n_tp):
+        gather_copy(0, tok, d).start()
+    for copy in loads[5:]:
+        copy.wait()
+
+    @pl.when(j == 0)
+    def _():
+        for s in range(1, stages):
+            own(s, UP)
+
+    @pl.when(j == n_fs - 1)
+    def _():
+        for s in range(1, stages):
+            own(s, DOWN)
+
+    def norm(buffer, gain):
+        squares = jnp.zeros((rows, 1), jnp.float32)
+        for b in range(n_tp):
+            values = buffer[b].astype(jnp.float32)
+            squares = squares + jnp.sum(values * values, axis=-1, keepdims=True)
+        scale = lax.rsqrt(squares / (n_tp * own_cols) + 1e-06)
+        for b in range(n_tp):
+            cut = slice(b * own_cols, (b + 1) * own_cols)
+            values = buffer[b].astype(jnp.float32)
+            normed[:, cut] = (values * scale * gain[:, cut]).astype(jnp.bfloat16)
+
+    for d in range(1, n_tp):
+        gather_wait(0, tok, d)
+    norm(tok, mix_gain)
+
+    relay(0, False)
+    relay(1, False)
+    arrived(0)
+
+    def project(weight):
+        product = jnp.dot(normed[...], weight, preferred_element_type=jnp.float32)
+        return product.astype(jnp.bfloat16).astype(jnp.float32)
+
+    gated = project(mix_in[2]) * project(mix_in[0])
+    conv = conv_rows(gated, mix_taps[...], length)
+    mixed = (project(mix_in[1]) * conv).astype(jnp.bfloat16)
+    for b in range(n_fs):
+        total[:, b * shard : (b + 1) * shard] = jnp.dot(
+            mixed, mix_out[b], preferred_element_type=jnp.float32
+        )
+    for b in range(n_tp):
+        part[b] = total[:, b * own_cols : (b + 1) * own_cols].astype(jnp.bfloat16)
+    for d in range(1, n_tp):
+        scatter_copy(1, part, got, d).start()
+
+    relay(2, False)
+
+    def summed(phase, sent, received):
+        value = sent[k].astype(jnp.float32)
+        for d in range(1, n_tp):
+            scatter_copy(phase, sent, received, d).wait_recv()
+            value = value + received[d].astype(jnp.float32)
+        return value
+
+    res[k] = (tok[k].astype(jnp.float32) + summed(1, part, got)).astype(jnp.bfloat16)
+    for d in range(1, n_tp):
+        gather_copy(2, res, d).start()
+
+    relay(3, stages == 4)
+    for d in range(1, n_tp):
+        gather_wait(2, res, d)
+    norm(res, ffn_gain)
+    total[...] = jnp.zeros_like(total)
+
+    def feed(s):
+        arrived(s)
+        cut = pl.ds(pl.multiple_of((s - 1) * chans, chans), chans)
+        gate = conv_rows(project(ffn_in[s - 1, 0]), up_taps[0, :, cut], length) + up_bias[0:1, cut]
+        value = conv_rows(project(ffn_in[s - 1, 1]), up_taps[1, :, cut], length) + up_bias[1:2, cut]
+        hidden = (gate / (1.0 + jnp.exp(-gate)) * value).astype(jnp.bfloat16)
+        for b in range(n_fs):
+            total[:, b * shard : (b + 1) * shard] += jnp.dot(
+                hidden, ffn_out[s - 1, b], preferred_element_type=jnp.float32
+            )
+
+    @pl.loop(1, stages)
+    def _(s):
+        @pl.when(s + 3 < stages - 1)
+        def _():
+            relay(s + 3, False)
+
+        @pl.when(s + 3 == stages - 1)
+        def _():
+            relay(s + 3, True)
+
+        feed(s)
+
+    for b in range(n_tp):
+        part_ffn[b] = total[:, b * own_cols : (b + 1) * own_cols].astype(jnp.bfloat16)
+    for d in range(1, n_tp):
+        scatter_copy(3, part_ffn, got_ffn, d).start()
+    out[...] = (res[k].astype(jnp.float32) + summed(3, part_ffn, got_ffn)).astype(jnp.bfloat16)
+
+    for d in range(1, n_tp):
+        gather_copy(0, tok, d).wait_send()
+        scatter_copy(1, part, got, d).wait_send()
+        gather_copy(2, res, d).wait_send()
+        scatter_copy(3, part_ffn, got_ffn, d).wait_send()
+
+    def drain(s):
+        for d in range(n_fs):
+
+            @pl.when((j - d >= 0) & (j + 1 < n_fs))
+            def _():
+                for copy in z_copies(s, j - d, UP):
+                    copy.wait_send()
+
+            @pl.when((j + d < n_fs) & (j >= 1))
+            def _():
+                for copy in z_copies(s, j + d, DOWN):
+                    copy.wait_send()
+
+        for d in range(1, n_fs):
+            for copy in y_copies(s, lax.rem(j + d, n_fs), g):
+                copy.wait_send()
+
+    drain(0)
+    pl.loop(1, stages)(drain)
+
+
+def fused(n_fs, n_tp, *args):
+    tokens, w_signal, w_gate = args[0], args[2], args[8]
+    rows, cols = tokens.shape
+    shard, chans = w_signal.shape
+    stages = 1 + w_gate.shape[1] // chans
+    width = n_fs * shard
+    args = list(args)
+    args[1], args[7] = args[1].reshape(1, -1), args[7].reshape(1, -1)
+    in_vmem = {1, 5, 7, 10, 11}
+    wide = (n_tp, rows, cols)
+    copies = 2 * stages
+    dma = pltpu.SemaphoreType.DMA
+    return pl.pallas_call(
+        functools.partial(layer_kernel, n_fs, n_tp),
+        out_shape=jax.ShapeDtypeStruct((rows, cols), jnp.bfloat16),
+        in_specs=[
+            pl.BlockSpec(memory_space=pltpu.VMEM if i in in_vmem else pl.ANY)
+            for i in range(len(args))
+        ],
+        out_specs=pl.BlockSpec(memory_space=pltpu.VMEM),
+        scratch_shapes=[
+            pltpu.VMEM((3, width, chans), jnp.bfloat16),
+            pltpu.VMEM((n_fs, chans, shard), jnp.bfloat16),
+            pltpu.VMEM((stages - 1, 2, width, chans), jnp.bfloat16),
+            pltpu.VMEM((stages - 1, n_fs, chans, shard), jnp.bfloat16),
+            pltpu.VMEM(wide, jnp.bfloat16),
+            pltpu.VMEM(wide, jnp.bfloat16),
+            pltpu.VMEM((rows, width), jnp.bfloat16),
+            pltpu.VMEM((rows, width), jnp.float32),
+            pltpu.VMEM(wide, jnp.bfloat16),
+            pltpu.VMEM(wide, jnp.bfloat16),
+            pltpu.VMEM(wide, jnp.bfloat16),
+            pltpu.VMEM(wide, jnp.bfloat16),
+            dma((2, copies, n_fs)),
+            dma((copies, n_fs)),
+            dma((copies, n_fs)),
+            dma((copies, n_fs)),
+            dma((5 + 3 * (stages - 1),)),
+            dma((4, n_tp)),
+            dma((4, n_tp)),
+        ],
+        compiler_params=pltpu.CompilerParams(
+            collective_id=0, has_side_effects=True, vmem_limit_bytes=60 * 1024 * 1024
+        ),
+    )(*args)
+
+
 def solution(mesh):
+    n_fs, n_tp = mesh.shape["fs"], mesh.shape["tp"]
+    body = functools.partial(fused, n_fs, n_tp)
+    if n_fs > 8 or mesh.shape["grp"] != 2:
+        body = on_device
     placed = (
         P(("grp", "fs"), "tp"),
         P(),
@@ -104,5 +495,5 @@
         P("tp", "fs"),
     )
     return jax.shard_map(
-        on_device, mesh=mesh, in_specs=placed, out_specs=P(("grp", "fs"), "tp"), check_vma=False
-    )
+        body, mesh=mesh, in_specs=placed, out_specs=P(("grp", "fs"), "tp"), check_vma=False
+    )

time: 538 us -> 207 us (0.38)
  the two profiles are of different devices: /device:TPU:0 before, /device:TPU:9 now
where the time goes in v1:
time: 207 us
  Pallas kernels  203 us (98%)
  local copies, waits for them, and re-layouts  3.15 us (2%)
    pallas_call x1, Pallas kernels, fused(): pl.pallas_call(functools.partial(layer_kernel, n_fs, n_tp), out_shape=jax...  203 us

profile of v1, /device:TPU:9, one launch (start us, length us, event | category | flops | bytes accessed | tf_op | source)
XLA Modules:
  0.0 206.6 jit_solution(2590286927257891933)
XLA Ops:
  0.0 1.4 copy.14.up_taps
  1.4 203.4 %shard_map.127 = bf16[384,512]{1,0:T(8,128)(2,1)} custom-call(bf16[384,512]{1,0:T(8,128)(2,1)} %tokens.1, f32[1,2048]{1,0:T(1,128)} %bitcast.2, bf16[512,256]{1,0:T(8,128)(2,1)} %w_signal.1, bf16[512,256]{1,0:T(8,128)(2,1)} %w_outer_gate.1, bf16[512,256]{1,0:T(8,128)(2,1)} %w_inner_gate.1, f32[3,256]{1,0:T(4,128)} %mix_taps.1, bf16[256,512]{1,0:T(8,128)(2,1)} %w_mix_out.1, ...), custom_call_target="tpu_custom_call" | custom-call | tf_op jit(solution)/shard_map/pallas_call | solution.py:442
  204.8 1.8 copy.16

commit v2 on v1

v2 whole, which is shorter than its diff:
```python
import functools

import jax
import jax.numpy as jnp
from jax import lax
from jax.experimental import pallas as pl
from jax.experimental.pallas import tpu as pltpu
from jax.sharding import PartitionSpec as P

SEQS_DEV = 2


def conv_positions(values, taps):
    width = values.shape[1]
    blocks = values.reshape(SEQS_DEV, -1, width)
    length = blocks.shape[1]
    padded = jnp.pad(blocks, ((0, 0), (2, 0), (0, 0)))
    result = (
        padded[:, 0:length] * taps[0]
        + padded[:, 1 : length + 1] * taps[1]
        + padded[:, 2 : length + 2] * taps[2]
    )
    return result.reshape(-1, width)


def rms_norm(stream, gain):
    values = stream.astype(jnp.float32)
    scale = lax.rsqrt(jnp.mean(values * values, axis=-1, keepdims=True) + 1e-06)
    return (values * scale * gain).astype(jnp.bfloat16)


def on_device(
    tokens,
    mix_gain,
    w_signal,
    w_outer_gate,
    w_inner_gate,
    mix_taps,
    w_mix_out,
    ffn_gain,
    w_gate,
    w_value,
    up_taps,
    up_bias,
    w_down,
):
    whole = lax.all_gather(tokens, "tp", axis=1, tiled=True)
    normed = rms_norm(whole, mix_gain)
    pieces = (
        lax.all_gather(w_signal, "fs", axis=0, tiled=True),
        lax.all_gather(w_outer_gate, "fs", axis=0, tiled=True),
        lax.all_gather(w_inner_gate, "fs", axis=0, tiled=True),
    )
    columns = normed
    signal, outer, inner = tuple(
        (jnp.dot(columns, piece, preferred_element_type=jnp.float32) for piece in pieces)
    )
    signal = signal.astype(jnp.bfloat16).astype(jnp.float32)
    outer = outer.astype(jnp.bfloat16).astype(jnp.float32)
    inner = inner.astype(jnp.bfloat16).astype(jnp.float32)
    mixed = (outer * conv_positions(inner * signal, mix_taps)).astype(jnp.bfloat16)
    mix_terms = jnp.dot(
        mixed,
        lax.all_gather(w_mix_out, "fs", axis=1, tiled=True),
        preferred_element_type=jnp.float32,
    )
    mix_sum = lax.psum_scatter(
        mix_terms.astype(jnp.bfloat16), "tp", scatter_dimension=1, tiled=True
    ).astype(jnp.float32)
    resid = (tokens.astype(jnp.float32) + mix_sum).astype(jnp.bfloat16)
    whole_ffn = lax.all_gather(resid, "tp", axis=1, tiled=True)
    normed_ffn = rms_norm(whole_ffn, ffn_gain)
    pieces = (
        lax.all_gather(w_gate, "fs", axis=0, tiled=True),
        lax.all_gather(w_value, "fs", axis=0, tiled=True),
    )
    columns = normed_ffn
    gate = jnp.dot(columns, pieces[0], preferred_element_type=jnp.float32)
    value = jnp.dot(columns, pieces[1], preferred_element_type=jnp.float32)
    gate = gate.astype(jnp.bfloat16).astype(jnp.float32)
    value = value.astype(jnp.bfloat16).astype(jnp.float32)
    gate_conv = conv_positions(gate, up_taps[0]) + up_bias[0]
    value_conv = conv_positions(value, up_taps[1]) + up_bias[1]
    hidden = (jax.nn.silu(gate_conv) * value_conv).astype(jnp.bfloat16)
    ffn_terms = jnp.dot(
        hidden, lax.all_gather(w_down, "fs", axis=1, tiled=True), preferred_element_type=jnp.float32
    )
    ffn_sum = lax.psum_scatter(
        ffn_terms.astype(jnp.bfloat16), "tp", scatter_dimension=1, tiled=True
    ).astype(jnp.float32)
    return (resid.astype(jnp.float32) + ffn_sum).astype(jnp.bfloat16)


MESH = pl.DeviceIdType.MESH
UP, DOWN = 0, 1
LANES = 128


def shifted(values, by, length):
    rolled = pltpu.roll(values, by, 0)
    position = lax.rem(lax.broadcasted_iota(jnp.int32, values.shape, 0), length)
    return jnp.where(position < by, 0.0, rolled)


def conv_rows(values, taps, length):
    return (
        shifted(values, 2, length) * taps[0:1]
        + shifted(values, 1, length) * taps[1:2]
        + values * taps[2:3]
    )


def layer_kernel(
    n_fs,
    n_tp,
    tokens,
    mix_gain,
    w_signal,
    w_outer_gate,
    w_inner_gate,
    mix_taps,
    w_mix_out,
    ffn_gain,
    w_gate,
    w_value,
    up_taps,
    up_bias,
    w_down,
    out,
    mix_in,
    mix_out,
    ffn_in,
    ffn_out,
    tok,
    res,
    normed,
    total,
    part,
    got,
    part_ffn,
    got_core,
    sum_x,
    got_x,
    sum_z,
    got_z,
    z_send,
    z_recv,
    y_send,
    y_recv,
    load_sem,
    tp_send,
    tp_recv,
    all_send,
    all_recv,
    core_send,
    core_recv,
    x_send,
    x_recv,
    pair_send,
    pair_recv,
):
    g, j, k = lax.axis_index("grp"), lax.axis_index("fs"), lax.axis_index("tp")
    rows, own_cols = tokens.shape
    length = rows // SEQS_DEV
    shard, chans = w_signal.shape
    half = shard // 2
    hidden_half = w_gate.shape[1] // 2
    stages = 1 + hidden_half // LANES
    n_x = n_tp // 2
    x, c = k // 2, lax.rem(k, 2)
    core = k + 1 - 2 * c
    p = lax.rem(j, 2)
    pair = j + 1 - 2 * p
    mine = pl.ds(pl.multiple_of(p * rows, rows), rows)
    theirs = pl.ds(pl.multiple_of((1 - p) * rows, rows), rows)

    def chunks(s):
        return (None,) if isinstance(s, int) and s == 0 else (0, 1)

    def top(q):
        return n_fs - 1 if q is None or (n_fs - 1) % 2 == q else n_fs - 2

    def bottom(q):
        return 0 if q is None else q

    def views(s, q, source, side):
        at_rows = pl.ds(pl.multiple_of((source * 2 + side) * half, half), half)
        tall = chans // 2 if q is None else LANES // 2
        at_chans = pl.ds(pl.multiple_of(side * tall, tall), tall)
        if q is None:
            return mix_in.at[:, at_rows, :], mix_out.at[source, at_chans, :]
        return ffn_in.at[s - 1, q, at_rows, :], ffn_out.at[s - 1, q, source, at_chans, :]

    def slot(s, q, i):
        return i if q is None else 2 + (s - 1) * 4 + q * 2 + i

    def z_copies(s, q, source, way):
        return [
            pltpu.make_async_remote_copy(
                src_ref=view,
                dst_ref=view,
                send_sem=z_send.at[way, slot(s, q, i), source],
                recv_sem=z_recv.at[slot(s, q, i), source],
                device_id={"fs": j + 1 if way == UP else j - 1},
                device_id_type=MESH,
            )
            for i, view in enumerate(views(s, q, source, g))
        ]

    def y_copies(s, q, source, side):
        return [
            pltpu.make_async_remote_copy(
                src_ref=view,
                dst_ref=view,
                send_sem=y_send.at[slot(s, q, i), source],
                recv_sem=y_recv.at[slot(s, q, i), source],
                device_id={"grp": 1 - g},
                device_id_type=MESH,
            )
            for i, view in enumerate(views(s, q, source, side))
        ]

    def start(copies):
        for copy in copies:
            copy.start()

    def wait_recv(copies):
        for copy in copies:
            copy.wait_recv()

    def wait_send(copies):
        for copy in copies:
            copy.wait_send()

    def goes_on(q, way):
        return j + 1 <= top(q) if way == UP else j - 1 >= bottom(q)

    def comes(q, source, way):
        if way == UP:
            return (source >= 0) & (j <= top(q))
        return (source < n_fs) & (j >= bottom(q))

    def own(s, way):
        for q in chunks(s):

            @pl.when(goes_on(q, way))
            def _():
                start(z_copies(s, q, j, way))

    def relay(s, last):
        for d in range(1, n_fs):
            for q in chunks(s):
                for way, source in ((UP, j - d), (DOWN, j + d)):

                    @pl.when(comes(q, source, way))
                    def _():
                        wait_recv(z_copies(s, q, source, way))

                        @pl.when(goes_on(q, way))
                        def _():
                            start(z_copies(s, q, source, way))

                        if q is None:
                            start(y_copies(s, q, source, g))
                        else:

                            @pl.when(p == q)
                            def _():
                                start(y_copies(s, q, source, g))

            if not last:

                @pl.when((j == d) & (j + 1 < n_fs))
                def _():
                    own(s + 1, UP)

                @pl.when((n_fs - 1 - j == d) & (j >= 1))
                def _():
                    own(s + 1, DOWN)

    def arrived(s):
        q = None if isinstance(s, int) and s == 0 else p
        for d in range(1, n_fs):
            wait_recv(y_copies(s, q, lax.rem(j + d, n_fs), 1 - g))

    def to_tp(src, dst, send_sem, recv_sem, to):
        return pltpu.make_async_remote_copy(
            src_ref=src,
            dst_ref=dst,
            send_sem=send_sem,
            recv_sem=recv_sem,
            device_id={"tp": to},
            device_id_type=MESH,
        )

    def tok_copy(d, source):
        return to_tp(
            tok.at[source], tok.at[source], tp_send.at[0, d], tp_recv.at[0, d], lax.rem(k + d, n_tp)
        )

    def mix_copy(d):
        to = lax.rem(k + d, n_tp)
        return to_tp(part.at[to], got.at[d], tp_send.at[1, d], tp_recv.at[1, d], to)

    def all_copies(o, at, kind):
        copies = []
        for dx in range(n_x):
            there = lax.rem(x + dx, n_x)
            if kind == "over":
                if dx:
                    view = res.at[k, at]
                    copies.append(
                        to_tp(
                            view,
                            view,
                            all_send.at[o, 0, dx],
                            all_recv.at[o, 0, dx],
                            there * 2 + c,
                        )
                    )
            else:
                back = lax.rem(x + n_x - dx, n_x) * 2
                seen = back + c if kind == "pass" else back + 1 - c
                view = res.at[seen, at]
                copies.append(
                    to_tp(view, view, all_send.at[o, 1, dx], all_recv.at[o, 1, dx], core)
                )
        return copies

    def all_begin(o, at):
        start(all_copies(o, at, "over"))
        all_copies(o, at, "pass")[0].start()

    def all_middle(o, at):
        passed = all_copies(o, at, "pass")
        for dx in range(1, n_x):
            view = res.at[lax.rem(x + n_x - dx, n_x) * 2 + c, at]
            to_tp(
                view, view, all_send.at[o, 0, dx], all_recv.at[o, 0, dx], core
            ).wait_recv()
            passed[dx].start()

    def all_end(o, at):
        wait_recv(all_copies(o, at, "take"))

    def to_pair(i, src, dst):
        return pltpu.make_async_remote_copy(
            src_ref=src,
            dst_ref=dst,
            send_sem=pair_send.at[i],
            recv_sem=pair_recv.at[i],
            device_id={"fs": pair},
            device_id_type=MESH,
        )

    barrier = pltpu.get_barrier_semaphore()
    for peer in (lax.rem(j + 1, n_fs), lax.rem(j + n_fs - 1, n_fs)):
        pl.semaphore_signal(barrier, inc=1, device_id={"fs": peer}, device_id_type=MESH)
    pl.semaphore_signal(barrier, inc=1, device_id={"grp": 1 - g}, device_id_type=MESH)
    for d in range(1, n_tp):
        pl.semaphore_signal(
            barrier, inc=1, device_id={"tp": lax.rem(k + d, n_tp)}, device_id_type=MESH
        )

    at_rows = pl.ds(pl.multiple_of(j * shard, shard), shard)
    loads = [
        pltpu.make_async_copy(ref, mix_in.at[i, at_rows, :], load_sem.at[i])
        for i, ref in enumerate((w_signal, w_outer_gate, w_inner_gate))
    ]
    loads.append(pltpu.make_async_copy(w_mix_out, mix_out.at[j], load_sem.at[3]))
    loads.append(pltpu.make_async_copy(tokens, tok.at[k], load_sem.at[4]))
    for s in range(1, stages):
        for q in (0, 1):
            cut = pl.ds(q * hidden_half + (s - 1) * LANES, LANES)
            for src, dst in (
                (w_gate.at[:, cut], ffn_in.at[s - 1, q, at_rows, pl.ds(0, LANES)]),
                (w_value.at[:, cut], ffn_in.at[s - 1, q, at_rows, pl.ds(LANES, LANES)]),
                (w_down.at[cut, :], ffn_out.at[s - 1, q, j]),
            ):
                loads.append(pltpu.make_async_copy(src, dst, load_sem.at[len(loads)]))
    start(loads)
    for copy in loads[:5]:
        copy.wait()
    pl.semaphore_wait(barrier, 3 + n_tp - 1)

    own(0, UP)
    own(0, DOWN)
    for d in range(1, n_tp):
        tok_copy(d, k).start()
    for copy in loads[5:]:
        copy.wait()

    @pl.when(j == 0)
    def _():
        for s in range(1, stages):
            own(s, UP)

    @pl.when(j == n_fs - 1)
    def _():
        for s in range(1, stages):
            own(s, DOWN)

    def norm(buffer, at, gain):
        squares = jnp.zeros((rows, 1), jnp.float32)
        for b in range(n_tp):
            values = buffer[b, at, :].astype(jnp.float32)
            squares = squares + jnp.sum(values * values, axis=-1, keepdims=True)
        scale = lax.rsqrt(squares / (n_tp * own_cols) + 1e-06)
        for b in range(n_tp):
            cut = slice(b * own_cols, (b + 1) * own_cols)
            values = buffer[b, at, :].astype(jnp.float32)
            normed[at, cut] = (values * scale * gain[:, cut]).astype(jnp.bfloat16)

    first = pl.ds(0, rows)
    for d in range(1, n_tp):
        tok_copy(d, lax.rem(k + n_tp - d, n_tp)).wait_recv()
    norm(tok, first, mix_gain)

    relay(0, False)
    arrived(0)

    def project(weight):
        product = jnp.dot(normed[first, :], weight, preferred_element_type=jnp.float32)
        return product.astype(jnp.bfloat16).astype(jnp.float32)

    gated = project(mix_in[2]) * project(mix_in[0])
    conv = conv_rows(gated, mix_taps[...], length)
    mixed = (project(mix_in[1]) * conv).astype(jnp.bfloat16)
    for b in range(n_fs):
        total[first, b * shard : (b + 1) * shard] = jnp.dot(
            mixed, mix_out[b], preferred_element_type=jnp.float32
        )
    for b in range(n_tp):
        part[b] = total[first, b * own_cols : (b + 1) * own_cols].astype(jnp.bfloat16)
    for d in range(1, n_tp):
        mix_copy(d).start()

    relay(1, False)

    mixer = part[k].astype(jnp.float32)
    for d in range(1, n_tp):
        mix_copy(d).wait_recv()
        mixer = mixer + got[d].astype(jnp.float32)
    res[k, mine, :] = (tok[k].astype(jnp.float32) + mixer).astype(jnp.bfloat16)
    swap = to_pair(0, res.at[k, mine], res.at[k, mine])
    swapped = to_pair(0, res.at[k, theirs], res.at[k, theirs])
    swap.start()
    all_begin(0, mine)

    relay(2, False)
    all_middle(0, mine)
    swapped.wait_recv()
    all_begin(1, theirs)
    all_end(0, mine)
    norm(res, mine, ffn_gain)
    relay(3, False)
    all_middle(1, theirs)
    all_end(1, theirs)
    norm(res, theirs, ffn_gain)
    total[...] = jnp.zeros_like(total)

    def feed(s):
        arrived(s)
        at = pl.multiple_of(p * hidden_half + (s - 1) * LANES, LANES)
        cut = pl.ds(at, LANES)
        both = jnp.dot(normed[...], ffn_in[s - 1, p], preferred_element_type=jnp.float32)
        both = both.astype(jnp.bfloat16).astype(jnp.float32)
        gate = conv_rows(both[:, :LANES], up_taps[0, :, cut], length) + up_bias[0:1, cut]
        value = conv_rows(both[:, LANES:], up_taps[1, :, cut], length) + up_bias[1:2, cut]
        hidden = (gate / (1.0 + jnp.exp(-gate)) * value).astype(jnp.bfloat16)
        for b in range(n_fs):
            total[:, b * shard : (b + 1) * shard] += jnp.dot(
                hidden, ffn_out[s - 1, p, b], preferred_element_type=jnp.float32
            )

    @pl.loop(1, stages)
    def _(s):
        @pl.when(s + 3 < stages - 1)
        def _():
            relay(s + 3, False)

        @pl.when(s + 3 == stages - 1)
        def _():
            relay(s + 3, True)

        feed(s)

    def core_copy(o, there, dx):
        return to_tp(
            part_ffn.at[o, there * 2 + 1 - c],
            got_core.at[o, there],
            core_send.at[o, dx],
            core_recv.at[o, dx],
            core,
        )

    def x_copy(o, dx):
        to = lax.rem(x + dx, n_x) * 2 + c
        return to_tp(sum_x.at[o, dx], got_x.at[o, dx], x_send.at[o, dx], x_recv.at[o, dx], to)

    order = [*range(1, n_x), 0]
    for o, at in enumerate((theirs, mine)):
        for b in range(n_tp):
            part_ffn[o, b] = total[at, b * own_cols : (b + 1) * own_cols].astype(jnp.bfloat16)
        for dx in order:
            core_copy(o, lax.rem(x + dx, n_x), dx).start()

    def chip_sum(o, dx):
        there = lax.rem(x + dx, n_x)
        core_copy(o, there, dx).wait_recv()
        return part_ffn[o, there * 2 + c].astype(jnp.float32) + got_core[o, there].astype(jnp.float32)

    for o in (0, 1):
        for dx in range(1, n_x):
            sum_x[o, dx] = chip_sum(o, dx).astype(jnp.bfloat16)
            x_copy(o, dx).start()

    def place_sum(o):
        value = chip_sum(o, 0)
        for dx in range(1, n_x):
            x_copy(o, dx).wait_recv()
            value = value + got_x[o, dx].astype(jnp.float32)
        return value

    sum_z[...] = place_sum(0).astype(jnp.bfloat16)
    back = to_pair(1, sum_z, got_z)
    back.start()
    value = res[k, mine, :].astype(jnp.float32) + place_sum(1)
    back.wait_recv()
    out[...] = (value + got_z[...].astype(jnp.float32)).astype(jnp.bfloat16)

    for d in range(1, n_tp):
        tok_copy(d, k).wait_send()
        mix_copy(d).wait_send()
    for o, at in enumerate((mine, theirs)):
        wait_send(all_copies(o, at, "over"))
        wait_send(all_copies(o, at, "pass"))
    for o in (0, 1):
        for dx in range(n_x):
            core_copy(o, lax.rem(x + dx, n_x), dx).wait_send()
        for dx in range(1, n_x):
            x_copy(o, dx).wait_send()
    swap.wait_send()
    back.wait_send()

    def drain(s):
        for q in chunks(s):
            for d in range(n_fs):
                for way, source in ((UP, j - d), (DOWN, j + d)):

                    @pl.when(comes(q, source, way) & goes_on(q, way))
                    def _():
                        wait_send(z_copies(s, q, source, way))

        q = None if isinstance(s, int) and s == 0 else p
        for d in range(1, n_fs):
            wait_send(y_copies(s, q, lax.rem(j + d, n_fs), g))

    drain(0)
    pl.loop(1, stages)(drain)


def fused(n_fs, n_tp, *args):
    tokens, w_signal, w_gate = args[0], args[2], args[8]
    rows, cols = tokens.shape
    shard, chans = w_signal.shape
    stages = 1 + w_gate.shape[1] // (2 * LANES)
    width = n_fs * shard
    args = list(args)
    args[1], args[7] = args[1].reshape(1, -1), args[7].reshape(1, -1)
    in_vmem = {1, 5, 7, 10, 11}
    n_x = n_tp // 2
    copies = 2 + 4 * (stages - 1)
    dma = pltpu.SemaphoreType.DMA

    def held(*shape):
        return pltpu.VMEM(shape, jnp.bfloat16)

    return pl.pallas_call(
        functools.partial(layer_kernel, n_fs, n_tp),
        out_shape=jax.ShapeDtypeStruct((rows, cols), jnp.bfloat16),
        in_specs=[
            pl.BlockSpec(memory_space=pltpu.VMEM if i in in_vmem else pl.ANY)
            for i in range(len(args))
        ],
        out_specs=pl.BlockSpec(memory_space=pltpu.VMEM),
        scratch_shapes=[
            held(3, width, chans),
            held(n_fs, chans, shard),
            held(stages - 1, 2, width, 2 * LANES),
            held(stages - 1, 2, n_fs, LANES, shard),
            held(n_tp, rows, cols),
            held(n_tp, 2 * rows, cols),
            held(2 * rows, width),
            pltpu.VMEM((2 * rows, width), jnp.float32),
            held(n_tp, rows, cols),
            held(n_tp, rows, cols),
            held(2, n_tp, rows, cols),
            held(2, n_x, rows, cols),
            held(2, n_x, rows, cols),
            held(2, n_x, rows, cols),
            held(rows, cols),
            held(rows, cols),
            dma((2, copies, n_fs)),
            dma((copies, n_fs)),
            dma((copies, n_fs)),
            dma((copies, n_fs)),
            dma((5 + 6 * (stages - 1),)),
            dma((2, n_tp)),
            dma((2, n_tp)),
            dma((2, 2, n_x)),
            dma((2, 2, n_x)),
            dma((2, n_x)),
            dma((2, n_x)),
            dma((2, n_x)),
            dma((2, n_x)),
            dma((2,)),
            dma((2,)),
        ],
        compiler_params=pltpu.CompilerParams(
            collective_id=0, has_side_effects=True, vmem_limit_bytes=62 * 1024 * 1024
        ),
    )(*args)


def solution(mesh):
    n_fs, n_tp = mesh.shape["fs"], mesh.shape["tp"]
    body = functools.partial(fused, n_fs, n_tp)
    if n_fs > 8 or n_fs % 2 or n_tp % 2 or mesh.shape["grp"] != 2:
        body = on_device
    placed = (
        P(("grp", "fs"), "tp"),
        P(),
        P("fs", "tp"),
        P("fs", "tp"),
        P("fs", "tp"),
        P(None, "tp"),
        P("tp", "fs"),
        P(),
        P("fs", "tp"),
        P("fs", "tp"),
        P(None, None, "tp"),
        P(None, "tp"),
        P("tp", "fs"),
    )
    return jax.shard_map(
        body, mesh=mesh, in_specs=placed, out_specs=P(("grp", "fs"), "tp"), check_vma=False
    )
```

time: 207 us -> 184 us (0.89)
  the two profiles are of different devices: /device:TPU:9 before, /device:TPU:0 now
where the time goes in v2:
time: 184 us; the launch traced here: 182 us
  Pallas kernels  178 us (97%)
  local copies, waits for them, and re-layouts  3.15 us (2%)
    pallas_call x1, Pallas kernels, fused(): pl.pallas_call(functools.partial(layer_kernel, n_fs, n_tp), out_shape=jax...  178 us

profile of v2, /device:TPU:0, one launch (start us, length us, event | category | flops | bytes accessed | tf_op | source)
XLA Modules:
  0.0 181.5 jit_solution(8880359441648864483)
XLA Ops:
  0.0 1.4 copy.14.up_taps
  1.4 178.4 %shard_map.127 = bf16[384,512]{1,0:T(8,128)(2,1)} custom-call(bf16[384,512]{1,0:T(8,128)(2,1)} %tokens.1, f32[1,2048]{1,0:T(1,128)} %bitcast.2, bf16[512,256]{1,0:T(8,128)(2,1)} %w_signal.1, bf16[512,256]{1,0:T(8,128)(2,1)} %w_outer_gate.1, bf16[512,256]{1,0:T(8,128)(2,1)} %w_inner_gate.1, f32[3,256]{1,0:T(4,128)} %mix_taps.1, bf16[256,512]{1,0:T(8,128)(2,1)} %w_mix_out.1, ...), custom_call_target="tpu_custom_call" | custom-call | tf_op jit(solution)/shard_map/pallas_call | solution.py:579
  179.8 1.8 copy.16

commit v3 on v2

--- a/solution.py
+++ b/solution.py
@@ -134,7 +134,7 @@
     tok,
     res,
     normed,
-    total,
+    hidden,
     part,
     got,
     part_ffn,
@@ -165,7 +165,7 @@
     shard, chans = w_signal.shape
     half = shard // 2
     hidden_half = w_gate.shape[1] // 2
-    stages = 1 + hidden_half // LANES
+    n_in, n_out = hidden_half // LANES, shard // LANES
     n_x = n_tp // 2
     x, c = k // 2, lax.rem(k, 2)
     core = k + 1 - 2 * c
@@ -174,8 +174,11 @@
     mine = pl.ds(pl.multiple_of(p * rows, rows), rows)
     theirs = pl.ds(pl.multiple_of((1 - p) * rows, rows), rows)
 
-    def chunks(s):
-        return (None,) if isinstance(s, int) and s == 0 else (0, 1)
+    mix = ("mix", 0)
+    order = [mix, *(("in", t) for t in range(n_in)), *(("out", u) for u in range(n_out))]
+
+    def chunks(stage):
+        return (None,) if stage[0] == "mix" else (0, 1)
 
     def top(q):
         return n_fs - 1 if q is None or (n_fs - 1) % 2 == q else n_fs - 2
@@ -183,16 +186,23 @@
     def bottom(q):
         return 0 if q is None else q
 
-    def views(s, q, source, side):
+    def views(stage, q, source, side):
+        kind, i = stage
         at_rows = pl.ds(pl.multiple_of((source * 2 + side) * half, half), half)
-        tall = chans // 2 if q is None else LANES // 2
+        tall = (chans if kind == "mix" else hidden_half) // 2
         at_chans = pl.ds(pl.multiple_of(side * tall, tall), tall)
-        if q is None:
+        if kind == "mix":
             return mix_in.at[:, at_rows, :], mix_out.at[source, at_chans, :]
-        return ffn_in.at[s - 1, q, at_rows, :], ffn_out.at[s - 1, q, source, at_chans, :]
-
-    def slot(s, q, i):
-        return i if q is None else 2 + (s - 1) * 4 + q * 2 + i
+        if kind == "in":
+            return (ffn_in.at[i, q, at_rows, :],)
+        lanes = pl.ds(pl.multiple_of(source * LANES, LANES), LANES)
+        return (ffn_out.at[i, q, at_chans, lanes],)
+
+    def slot(stage, q, i):
+        kind, at = stage
+        if kind == "mix":
+            return i
+        return 2 + 2 * (at if kind == "in" else at + n_in) + q
 
     def z_copies(s, q, source, way):
         return [
@@ -247,7 +257,9 @@
             def _():
                 start(z_copies(s, q, j, way))
 
-    def relay(s, last):
+    def relay(s):
+        at = order.index(s)
+        following = order[at + 1] if at + 1 < len(order) else None
         for d in range(1, n_fs):
             for q in chunks(s):
                 for way, source in ((UP, j - d), (DOWN, j + d)):
@@ -268,18 +280,18 @@
                             def _():
                                 start(y_copies(s, q, source, g))
 
-            if not last:
+            if following:
 
                 @pl.when((j == d) & (j + 1 < n_fs))
                 def _():
-                    own(s + 1, UP)
+                    own(following, UP)
 
                 @pl.when((n_fs - 1 - j == d) & (j >= 1))
                 def _():
-                    own(s + 1, DOWN)
+                    own(following, DOWN)
 
     def arrived(s):
-        q = None if isinstance(s, int) and s == 0 else p
+        q = None if s[0] == "mix" else p
         for d in range(1, n_fs):
             wait_recv(y_copies(s, q, lax.rem(j + d, n_fs), 1 - g))
 
@@ -369,22 +381,24 @@
     ]
     loads.append(pltpu.make_async_copy(w_mix_out, mix_out.at[j], load_sem.at[3]))
     loads.append(pltpu.make_async_copy(tokens, tok.at[k], load_sem.at[4]))
-    for s in range(1, stages):
-        for q in (0, 1):
-            cut = pl.ds(q * hidden_half + (s - 1) * LANES, LANES)
-            for src, dst in (
-                (w_gate.at[:, cut], ffn_in.at[s - 1, q, at_rows, pl.ds(0, LANES)]),
-                (w_value.at[:, cut], ffn_in.at[s - 1, q, at_rows, pl.ds(LANES, LANES)]),
-                (w_down.at[cut, :], ffn_out.at[s - 1, q, j]),
-            ):
-                loads.append(pltpu.make_async_copy(src, dst, load_sem.at[len(loads)]))
+    for q in (0, 1):
+        for t in range(n_in):
+            at = pl.ds(q * hidden_half + t * LANES, LANES)
+            for i, ref in enumerate((w_gate, w_value)):
+                dst = ffn_in.at[t, q, at_rows, pl.ds(i * LANES, LANES)]
+                loads.append(pltpu.make_async_copy(ref.at[:, at], dst, load_sem.at[len(loads)]))
+        for u in range(n_out):
+            src = w_down.at[pl.ds(q * hidden_half, hidden_half), pl.ds(u * LANES, LANES)]
+            lanes = pl.ds(pl.multiple_of(j * LANES, LANES), LANES)
+            dst = ffn_out.at[u, q, :, lanes]
+            loads.append(pltpu.make_async_copy(src, dst, load_sem.at[len(loads)]))
     start(loads)
     for copy in loads[:5]:
         copy.wait()
     pl.semaphore_wait(barrier, 3 + n_tp - 1)
 
-    own(0, UP)
-    own(0, DOWN)
+    own(mix, UP)
+    own(mix, DOWN)
     for d in range(1, n_tp):
         tok_copy(d, k).start()
     for copy in loads[5:]:
@@ -392,12 +406,12 @@
 
     @pl.when(j == 0)
     def _():
-        for s in range(1, stages):
+        for s in order[1:]:
             own(s, UP)
 
     @pl.when(j == n_fs - 1)
     def _():
-        for s in range(1, stages):
+        for s in order[1:]:
             own(s, DOWN)
 
     def norm(buffer, at, gain):
@@ -416,8 +430,8 @@
         tok_copy(d, lax.rem(k + n_tp - d, n_tp)).wait_recv()
     norm(tok, first, mix_gain)
 
-    relay(0, False)
-    arrived(0)
+    relay(mix)
+    arrived(mix)
 
     def project(weight):
         product = jnp.dot(normed[first, :], weight, preferred_element_type=jnp.float32)
@@ -427,15 +441,11 @@
     conv = conv_rows(gated, mix_taps[...], length)
     mixed = (project(mix_in[1]) * conv).astype(jnp.bfloat16)
     for b in range(n_fs):
-        total[first, b * shard : (b + 1) * shard] = jnp.dot(
-            mixed, mix_out[b], preferred_element_type=jnp.float32
-        )
-    for b in range(n_tp):
-        part[b] = total[first, b * own_cols : (b + 1) * own_cols].astype(jnp.bfloat16)
+        part[b] = jnp.dot(mixed, mix_out[b], preferred_element_type=jnp.float32).astype(jnp.bfloat16)
     for d in range(1, n_tp):
         mix_copy(d).start()
 
-    relay(1, False)
+    relay(order[1])
 
     mixer = part[k].astype(jnp.float32)
     for d in range(1, n_tp):
@@ -447,87 +457,107 @@
     swap.start()
     all_begin(0, mine)
 
-    relay(2, False)
+    relay(order[2])
     all_middle(0, mine)
     swapped.wait_recv()
     all_begin(1, theirs)
     all_end(0, mine)
     norm(res, mine, ffn_gain)
-    relay(3, False)
+    relay(order[3])
     all_middle(1, theirs)
     all_end(1, theirs)
     norm(res, theirs, ffn_gain)
-    total[...] = jnp.zeros_like(total)
-
-    def feed(s):
-        arrived(s)
-        at = pl.multiple_of(p * hidden_half + (s - 1) * LANES, LANES)
-        cut = pl.ds(at, LANES)
-        both = jnp.dot(normed[...], ffn_in[s - 1, p], preferred_element_type=jnp.float32)
+    relay(order[4])
+
+    def feed(t):
+        arrived(("in", t))
+        cut = pl.ds(pl.multiple_of(p * hidden_half + t * LANES, LANES), LANES)
+        both = jnp.dot(normed[...], ffn_in[t, p], preferred_element_type=jnp.float32)
         both = both.astype(jnp.bfloat16).astype(jnp.float32)
         gate = conv_rows(both[:, :LANES], up_taps[0, :, cut], length) + up_bias[0:1, cut]
         value = conv_rows(both[:, LANES:], up_taps[1, :, cut], length) + up_bias[1:2, cut]
-        hidden = (gate / (1.0 + jnp.exp(-gate)) * value).astype(jnp.bfloat16)
-        for b in range(n_fs):
-            total[:, b * shard : (b + 1) * shard] += jnp.dot(
-                hidden, ffn_out[s - 1, p, b], preferred_element_type=jnp.float32
-            )
-
-    @pl.loop(1, stages)
-    def _(s):
-        @pl.when(s + 3 < stages - 1)
-        def _():
-            relay(s + 3, False)
-
-        @pl.when(s + 3 == stages - 1)
-        def _():
-            relay(s + 3, True)
-
-        feed(s)
-
-    def core_copy(o, there, dx):
+        units = (gate / (1.0 + jnp.exp(-gate)) * value).astype(jnp.bfloat16)
+        hidden[:, pl.ds(pl.multiple_of(t * LANES, LANES), LANES)] = units
+
+    beside = {0: 5, 1: 6, 3: 7}
+
+    @pl.loop(0, n_in)
+    def _(t):
+        for at, index in beside.items():
+
+            @pl.when(t == at)
+            def _():
+                relay(order[index])
+
+        feed(t)
+
+    def core_copy(u, dx):
+        there = lax.rem(x + dx, n_x)
         return to_tp(
-            part_ffn.at[o, there * 2 + 1 - c],
-            got_core.at[o, there],
-            core_send.at[o, dx],
-            core_recv.at[o, dx],
+            part_ffn.at[u, :, there * 2 + 1 - c],
+            got_core.at[u, :, there],
+            core_send.at[u, dx],
+            core_recv.at[u, dx],
             core,
         )
 
-    def x_copy(o, dx):
+    def x_copy(u, dx):
         to = lax.rem(x + dx, n_x) * 2 + c
-        return to_tp(sum_x.at[o, dx], got_x.at[o, dx], x_send.at[o, dx], x_recv.at[o, dx], to)
-
-    order = [*range(1, n_x), 0]
-    for o, at in enumerate((theirs, mine)):
-        for b in range(n_tp):
-            part_ffn[o, b] = total[at, b * own_cols : (b + 1) * own_cols].astype(jnp.bfloat16)
-        for dx in order:
-            core_copy(o, lax.rem(x + dx, n_x), dx).start()
-
-    def chip_sum(o, dx):
+        return to_tp(sum_x.at[u, dx], got_x.at[u, dx], x_send.at[u, dx], x_recv.at[u, dx], to)
+
+    def back(u):
+        return to_pair(1 + u, sum_z.at[u], got_z.at[u])
+
+    def chip_sum(u, o, dx):
         there = lax.rem(x + dx, n_x)
-        core_copy(o, there, dx).wait_recv()
-        return part_ffn[o, there * 2 + c].astype(jnp.float32) + got_core[o, there].astype(jnp.float32)
-
-    for o in (0, 1):
+        mine_there = part_ffn[u, o, there * 2 + c].astype(jnp.float32)
+        return mine_there + got_core[u, o, there].astype(jnp.float32)
+
+    def place_sum(u, o):
+        value = chip_sum(u, o, 0)
         for dx in range(1, n_x):
-            sum_x[o, dx] = chip_sum(o, dx).astype(jnp.bfloat16)
-            x_copy(o, dx).start()
-
-    def place_sum(o):
-        value = chip_sum(o, 0)
+            value = value + got_x[u, dx, o].astype(jnp.float32)
+        return value
+
+    def down(u):
+        arrived(("out", u))
+        for o, at in enumerate((theirs, mine)):
+            terms = jnp.dot(hidden[at, :], ffn_out[u, p], preferred_element_type=jnp.float32)
+            for b in range(n_tp):
+                part_ffn[u, o, b] = terms[:, b * LANES : (b + 1) * LANES].astype(jnp.bfloat16)
+        for dx in (*range(1, n_x), 0):
+            core_copy(u, dx).start()
+
+    def over_x(u):
         for dx in range(1, n_x):
-            x_copy(o, dx).wait_recv()
-            value = value + got_x[o, dx].astype(jnp.float32)
-        return value
-
-    sum_z[...] = place_sum(0).astype(jnp.bfloat16)
-    back = to_pair(1, sum_z, got_z)
-    back.start()
-    value = res[k, mine, :].astype(jnp.float32) + place_sum(1)
-    back.wait_recv()
-    out[...] = (value + got_z[...].astype(jnp.float32)).astype(jnp.bfloat16)
+            core_copy(u, dx).wait_recv()
+            for o in (0, 1):
+                sum_x[u, dx, o] = chip_sum(u, o, dx).astype(jnp.bfloat16)
+            x_copy(u, dx).start()
+
+    def over_z(u):
+        core_copy(u, 0).wait_recv()
+        for dx in range(1, n_x):
+            x_copy(u, dx).wait_recv()
+        sum_z[u] = place_sum(u, 0).astype(jnp.bfloat16)
+        back(u).start()
+
+    for u in range(n_out):
+        if 8 + u < len(order):
+            relay(order[8 + u])
+        down(u)
+        if u >= 1:
+            over_x(u - 1)
+        if u >= 2:
+            over_z(u - 2)
+    over_x(n_out - 1)
+    for u in range(max(n_out - 2, 0), n_out):
+        over_z(u)
+    for u in range(n_out):
+        cut = slice(u * LANES, (u + 1) * LANES)
+        value = res[k, mine, cut].astype(jnp.float32) + place_sum(u, 1)
+        back(u).wait_recv()
+        out[:, cut] = (value + got_z[u].astype(jnp.float32)).astype(jnp.bfloat16)
 
     for d in range(1, n_tp):
         tok_copy(d, k).wait_send()
@@ -535,13 +565,13 @@
     for o, at in enumerate((mine, theirs)):
         wait_send(all_copies(o, at, "over"))
         wait_send(all_copies(o, at, "pass"))
-    for o in (0, 1):
+    for u in range(n_out):
         for dx in range(n_x):
-            core_copy(o, lax.rem(x + dx, n_x), dx).wait_send()
+            core_copy(u, dx).wait_send()
         for dx in range(1, n_x):
-            x_copy(o, dx).wait_send()
+            x_copy(u, dx).wait_send()
+        back(u).wait_send()
     swap.wait_send()
-    back.wait_send()
 
     def drain(s):
         for q in chunks(s):
@@ -552,25 +582,33 @@
                     def _():
                         wait_send(z_copies(s, q, source, way))
 
-        q = None if isinstance(s, int) and s == 0 else p
+        q = None if s[0] == "mix" else p
         for d in range(1, n_fs):
             wait_send(y_copies(s, q, lax.rem(j + d, n_fs), g))
 
-    drain(0)
-    pl.loop(1, stages)(drain)
+    drain(mix)
+
+    @pl.loop(0, n_in)
+    def _(t):
+        drain(("in", t))
+
+    @pl.loop(0, n_out)
+    def _(u):
+        drain(("out", u))
 
 
 def fused(n_fs, n_tp, *args):
     tokens, w_signal, w_gate = args[0], args[2], args[8]
     rows, cols = tokens.shape
     shard, chans = w_signal.shape
-    stages = 1 + w_gate.shape[1] // (2 * LANES)
+    hidden = w_gate.shape[1] // 2
+    n_in, n_out = hidden // LANES, shard // LANES
     width = n_fs * shard
     args = list(args)
     args[1], args[7] = args[1].reshape(1, -1), args[7].reshape(1, -1)
     in_vmem = {1, 5, 7, 10, 11}
     n_x = n_tp // 2
-    copies = 2 + 4 * (stages - 1)
+    copies = 2 + 2 * (n_in + n_out)
     dma = pltpu.SemaphoreType.DMA
 
     def held(*shape):
@@ -587,35 +625,35 @@
         scratch_shapes=[
             held(3, width, chans),
             held(n_fs, chans, shard),
-            held(stages - 1, 2, width, 2 * LANES),
-            held(stages - 1, 2, n_fs, LANES, shard),
+            held(n_in, 2, width, 2 * LANES),
+            held(n_out, 2, hidden, n_fs * LANES),
             held(n_tp, rows, cols),
             held(n_tp, 2 * rows, cols),
             held(2 * rows, width),
-            pltpu.VMEM((2 * rows, width), jnp.float32),
+            held(2 * rows, hidden),
             held(n_tp, rows, cols),
             held(n_tp, rows, cols),
-            held(2, n_tp, rows, cols),
-            held(2, n_x, rows, cols),
-            held(2, n_x, rows, cols),
-            held(2, n_x, rows, cols),
-            held(rows, cols),
-            held(rows, cols),
+            held(n_out, 2, n_tp, rows, LANES),
+            held(n_out, 2, n_x, rows, LANES),
+            held(n_out, n_x, 2, rows, LANES),
+            held(n_out, n_x, 2, rows, LANES),
+            held(n_out, rows, LANES),
+            held(n_out, rows, LANES),
             dma((2, copies, n_fs)),
             dma((copies, n_fs)),
             dma((copies, n_fs)),
             dma((copies, n_fs)),
-            dma((5 + 6 * (stages - 1),)),
+            dma((5 + 4 * n_in + 2 * n_out,)),
             dma((2, n_tp)),
             dma((2, n_tp)),
             dma((2, 2, n_x)),
             dma((2, 2, n_x)),
-            dma((2, n_x)),
-            dma((2, n_x)),
-            dma((2, n_x)),
-            dma((2, n_x)),
-            dma((2,)),
-            dma((2,)),
+            dma((n_out, n_x)),
+            dma((n_out, n_x)),
+            dma((n_out, n_x)),
+            dma((n_out, n_x)),
+            dma((1 + n_out,)),
+            dma((1 + n_out,)),
         ],
         compiler_params=pltpu.CompilerParams(
             collective_id=0, has_side_effects=True, vmem_limit_bytes=62 * 1024 * 1024
@@ -626,7 +664,7 @@
 def solution(mesh):
     n_fs, n_tp = mesh.shape["fs"], mesh.shape["tp"]
     body = functools.partial(fused, n_fs, n_tp)
-    if n_fs > 8 or n_fs % 2 or n_tp % 2 or mesh.shape["grp"] != 2:
+    if n_fs > 8 or n_fs != n_tp or n_fs % 2 or mesh.shape["grp"] != 2:
         body = on_device
     placed = (
         P(("grp", "fs"), "tp"),

time: 184 us -> 180 us (0.978)
  Pallas kernels: 178 us -> 176 us
    pallas_call x1, Pallas kernels: 178 us -> 176 us  [fused(): pl.pallas_call(functools.partial(layer_kernel, n_fs, n_tp), out_shape=jax...]
where the time goes in v3:
time: 180 us; the launch traced here: 179 us
  Pallas kernels  176 us (98%)
  local copies, waits for them, and re-layouts  3.15 us (2%)
    pallas_call x1, Pallas kernels, fused(): pl.pallas_call(functools.partial(layer_kernel, n_fs, n_tp), out_shape=jax...  176 us

profile of v3, /device:TPU:0, one launch (start us, length us, event | category | flops | bytes accessed | tf_op | source)
XLA Modules:
  0.0 179.2 jit_solution(17096157329236151995)
XLA Ops:
  0.0 1.4 copy.14.up_taps
  1.4 176.1 %shard_map.127 = bf16[384,512]{1,0:T(8,128)(2,1)} custom-call(bf16[384,512]{1,0:T(8,128)(2,1)} %tokens.1, f32[1,2048]{1,0:T(1,128)} %bitcast.2, bf16[512,256]{1,0:T(8,128)(2,1)} %w_signal.1, bf16[512,256]{1,0:T(8,128)(2,1)} %w_outer_gate.1, bf16[512,256]{1,0:T(8,128)(2,1)} %w_inner_gate.1, f32[3,256]{1,0:T(4,128)} %mix_taps.1, bf16[256,512]{1,0:T(8,128)(2,1)} %w_mix_out.1, ...), custom_call_target="tpu_custom_call" | custom-call | tf_op jit(solution)/shard_map/pallas_call | solution.py:617
  177.5 1.8 copy.16

commit v4 on v3

--- a/solution.py
+++ b/solution.py
@@ -259,7 +259,7 @@
 
     def relay(s):
         at = order.index(s)
-        following = order[at + 1] if at + 1 < len(order) else None
+        following = order[at + 2 : at + 3] if at else order[1:3]
         for d in range(1, n_fs):
             for q in chunks(s):
                 for way, source in ((UP, j - d), (DOWN, j + d)):
@@ -284,11 +284,13 @@
 
                 @pl.when((j == d) & (j + 1 < n_fs))
                 def _():
-                    own(following, UP)
+                    for later in following:
+                        own(later, UP)
 
                 @pl.when((n_fs - 1 - j == d) & (j >= 1))
                 def _():
-                    own(following, DOWN)
+                    for later in following:
+                        own(later, DOWN)
 
     def arrived(s):
         q = None if s[0] == "mix" else p
@@ -431,6 +433,7 @@
     norm(tok, first, mix_gain)
 
     relay(mix)
+    relay(order[1])
     arrived(mix)
 
     def project(weight):
@@ -445,7 +448,6 @@
     for d in range(1, n_tp):
         mix_copy(d).start()
 
-    relay(order[1])
 
     mixer = part[k].astype(jnp.float32)
     for d in range(1, n_tp):

time: 180 us -> 176 us (0.978)
  Pallas kernels: 176 us -> 172 us
    pallas_call x1, Pallas kernels: 176 us -> 172 us  [fused(): pl.pallas_call(functools.partial(layer_kernel, n_fs, n_tp), out_shape=jax...]
where the time goes in v4:
time: 176 us; the launch traced here: 175 us
  Pallas kernels  172 us (98%)
  local copies, waits for them, and re-layouts  3.15 us (2%)
    pallas_call x1, Pallas kernels, fused(): pl.pallas_call(functools.partial(layer_kernel, n_fs, n_tp), out_shape=jax...  172 us

profile of v4, /device:TPU:0, one launch (start us, length us, event | category | flops | bytes accessed | tf_op | source)
XLA Modules:
  0.0 174.7 jit_solution(9463818296446509466)
XLA Ops:
  0.0 1.4 copy.14.up_taps
  1.4 171.5 %shard_map.127 = bf16[384,512]{1,0:T(8,128)(2,1)} custom-call(bf16[384,512]{1,0:T(8,128)(2,1)} %tokens.1, f32[1,2048]{1,0:T(1,128)} %bitcast.2, bf16[512,256]{1,0:T(8,128)(2,1)} %w_signal.1, bf16[512,256]{1,0:T(8,128)(2,1)} %w_outer_gate.1, bf16[512,256]{1,0:T(8,128)(2,1)} %w_inner_gate.1, f32[3,256]{1,0:T(4,128)} %mix_taps.1, bf16[256,512]{1,0:T(8,128)(2,1)} %w_mix_out.1, ...), custom_call_target="tpu_custom_call" | custom-call | tf_op jit(solution)/shard_map/pallas_call | solution.py:619
  172.9 1.8 %copy.16 = bf16[384,512]{1,0:T(8,128)(2,1)} copy(bf16[384,512]{1,0:T(8,128)(2,1)} %shard_map.127) | data formatting | bytes 786432
